TPU v7x, 32 devices: a whole 2x2x4 slice. The times are simulated.
32 devices in a mesh: sp: 8 (over z, x), tp: 4 (over y, core).
Axes of the slice: x: 2, y: 2, z: 4, core: 2. Of those that a mesh axis runs over, the one named last changes fastest.
Arguments:
- features: bfloat16 [3072, 2048], P('sp', 'tp'), may hold values from -6 to 6
- norm_gain: float32 [2048], replicated, may hold values from 0.28 to 10
- w_query: bfloat16 [2048, 1024], P(None, 'tp'), may hold values from -0.125 to 0.125
- w_key: bfloat16 [2048, 512], P(None, 'tp'), may hold values from -0.125 to 0.125
- w_value: bfloat16 [2048, 512], P(None, 'tp'), may hold values from -0.125 to 0.125
- head_sinks: float32 [16], P('tp'), may hold values from 1 to 5
- w_query_latent: bfloat16 [2048, 512], replicated, may hold values from -0.125 to 0.125
- w_kv_latent: bfloat16 [2048, 512], replicated, may hold values from -0.125 to 0.125
- w_rope_key: bfloat16 [2048, 64], replicated, may hold values from -0.125 to 0.125
- query_latent_gain: float32 [512], replicated, may hold values from 0.28 to 10
- kv_latent_gain: float32 [512], replicated, may hold values from 0.28 to 10
- w_query_content: bfloat16 [512, 1024], P(None, 'tp'), may hold values from -0.25 to 0.25
- w_query_rotary: bfloat16 [512, 512], P(None, 'tp'), may hold values from -0.25 to 0.25
- w_key_up: bfloat16 [512, 1024], P(None, 'tp'), may hold values from -0.25 to 0.25
- w_value_up: bfloat16 [512, 1024], P(None, 'tp'), may hold values from -0.25 to 0.25
- w_branch_window: bfloat16 [1024, 2048], P('tp'), may hold values from -0.1875 to 0.1875
- w_branch_latent: bfloat16 [1024, 2048], P('tp'), may hold values from -0.1875 to 0.1875
- w_gate_window: bfloat16 [2048, 2048], P(None, 'tp'), may hold values from -0.125 to 0.125
- w_gate_latent: bfloat16 [2048, 2048], P(None, 'tp'), may hold values from -0.125 to 0.125
Outputs:
- mixed: bfloat16 [3072, 2048], P('sp', 'tp')
All inputs are finite; a program needn't handle non-finite values.
Results may differ from a plain program's by a relative error of at most 0.018.
The roundings to bfloat16 on the way count: a program that leaves them out, or rounds other values in their place, can miss the bound.
Values may be sent and summed in bfloat16 or wider, within the bound.
A program may use at most 128 MiB of HBM per device.

v0:
```python
import jax
import jax.numpy as jnp
from jax import lax
from jax.sharding import PartitionSpec as P

HEAD = 64
WINDOW = 128
NOPE = 128
ROPE = 64
VDIM = 128
EPS = 1e-06
THETA = 10000.0
NEGATIVE = -1e30


def from_behind(shard, axis, by):
    count = lax.axis_size(axis)
    pairs = [(i, i + by) for i in range(count) if 0 <= i + by < count]
    return lax.ppermute(shard, axis, pairs)


def rms_rows(float_rows, gain_vec):
    return (
        float_rows
        * lax.rsqrt(jnp.mean(float_rows * float_rows, axis=-1, keepdims=True) + EPS)
        * gain_vec
    )


def rotate(float_rows, positions):
    half_width = float_rows.shape[-1] // 2
    frequencies = THETA ** (-jnp.arange(half_width, dtype=jnp.float32) / half_width)
    angles = positions.astype(jnp.float32)[:, None] * frequencies
    target = (float_rows.shape[0],) + (1,) * (float_rows.ndim - 2) + (half_width,)
    cosine = jnp.cos(angles).reshape(target)
    sine_part = jnp.sin(angles).reshape(target)
    first_half = float_rows[..., :half_width]
    second_half = float_rows[..., half_width:]
    return jnp.concatenate(
        [
            first_half * cosine - second_half * sine_part,
            second_half * cosine + first_half * sine_part,
        ],
        axis=-1,
    )


def project(left, right):
    return jnp.dot(left, right, preferred_element_type=jnp.float32)


def window_attention(queries, key_ext, value_ext, sink_table, row_start):
    row_count = queries.shape[0]
    kv_heads = key_ext.shape[1] // HEAD
    group_size = queries.shape[1] // HEAD // kv_heads
    blocks = row_count // WINDOW
    query_blocks = queries.reshape(blocks, WINDOW, kv_heads, group_size, HEAD)

    def banded(table):
        table = table.reshape(blocks + 1, WINDOW, kv_heads, HEAD)
        return jnp.concatenate([table[:-1], table[1:]], axis=1)

    key_band = banded(key_ext)
    value_band = banded(value_ext)
    scores = jnp.einsum(
        "nqhgd,nkhd->nhgqk", query_blocks, key_band, preferred_element_type=jnp.float32
    ) * HEAD ** (-0.5)
    query_index = jnp.arange(WINDOW, dtype=jnp.int32)[:, None]
    key_index = jnp.arange(2 * WINDOW, dtype=jnp.int32)[None, :]
    offset = query_index + WINDOW - key_index
    key_position = (
        row_start + jnp.arange(blocks, dtype=jnp.int32)[:, None, None] * WINDOW + key_index - WINDOW
    )
    valid_mask = ((offset >= 0) & (offset < WINDOW) & (key_position >= 0))[:, None, None]
    scores = jnp.where(valid_mask, scores, NEGATIVE)
    sink_logit = sink_table.reshape(1, kv_heads, group_size, 1, 1)
    row_top = jnp.maximum(jnp.max(scores, axis=-1, keepdims=True), sink_logit)
    weights = jnp.where(valid_mask, jnp.exp(scores - row_top), 0.0)
    denominator = jnp.sum(weights, axis=-1, keepdims=True) + jnp.exp(sink_logit - row_top)
    probabilities = (weights / denominator).astype(jnp.bfloat16)
    attended = jnp.einsum(
        "nhgqk,nkhd->nqhgd", probabilities, value_band, preferred_element_type=jnp.float32
    )
    return attended.astype(jnp.bfloat16).reshape(row_count, kv_heads * group_size * HEAD)


def on_device(
    features,
    norm_gain,
    w_query,
    w_key,
    w_value,
    head_sinks,
    w_query_latent,
    w_kv_latent,
    w_rope_key,
    query_latent_gain,
    kv_latent_gain,
    w_query_content,
    w_query_rotary,
    w_key_up,
    w_value_up,
    w_branch_window,
    w_branch_latent,
    w_gate_window,
    w_gate_latent,
):
    tok_rows = features.shape[0]
    row_start = lax.axis_index("sp") * tok_rows
    row_end = row_start + tok_rows
    positions = row_start + jnp.arange(tok_rows, dtype=jnp.int32)
    gathered = lax.all_gather(features, "tp", axis=1, tiled=True)
    normed = rms_rows(gathered.astype(jnp.float32), norm_gain).astype(jnp.bfloat16)
    query_rows = project(normed, w_query).astype(jnp.bfloat16)
    key_rows = project(normed, w_key).astype(jnp.bfloat16)
    value_rows = project(normed, w_value).astype(jnp.bfloat16)
    key_width = key_rows.shape[1]
    packed = jnp.concatenate([key_rows, value_rows], axis=1)
    tail_rows = from_behind(packed[tok_rows - WINDOW :], "sp", 1)
    extended = jnp.concatenate([tail_rows, packed], axis=0)
    window_out = window_attention(
        query_rows, extended[:, :key_width], extended[:, key_width:], head_sinks, row_start
    )
    latent_query = rms_rows(project(normed, w_query_latent), query_latent_gain).astype(jnp.bfloat16)
    latent_kv = rms_rows(project(normed, w_kv_latent), kv_latent_gain).astype(jnp.bfloat16)
    rope_rows = rotate(project(normed, w_rope_key), positions).astype(jnp.bfloat16)
    lat_heads = w_key_up.shape[1] // NOPE
    query_content = (
        project(latent_query, w_query_content)
        .astype(jnp.bfloat16)
        .reshape(tok_rows, lat_heads, NOPE)
    )
    query_rotary = rotate(
        project(latent_query, w_query_rotary).reshape(tok_rows, lat_heads, ROPE), positions
    ).astype(jnp.bfloat16)
    scale_factor = (NOPE + ROPE) ** (-0.5)

    def attend(running, piece_keys, piece_values, rope_piece):
        running_max, denominator, accumulated = running
        piece_rows = piece_keys.shape[0]
        scores = (
            jnp.einsum(
                "qhd,khd->hqk",
                query_content,
                piece_keys.reshape(piece_rows, lat_heads, NOPE),
                preferred_element_type=jnp.float32,
            )
            + jnp.einsum(
                "qhr,kr->hqk", query_rotary, rope_piece, preferred_element_type=jnp.float32
            )
        ) * scale_factor
        key_position = jnp.arange(piece_rows, dtype=jnp.int32)
        live_mask = key_position[None, :] <= positions[:, None]
        scores = jnp.where(live_mask, scores, NEGATIVE)
        new_max = jnp.maximum(running_max, jnp.max(scores, axis=-1))
        weights = jnp.where(live_mask, jnp.exp(scores - new_max[..., None]), 0.0)
        denominator = jnp.sum(weights, axis=-1)
        accumulated = jnp.einsum(
            "hqk,khd->hqd",
            weights.astype(jnp.bfloat16),
            piece_values.reshape(piece_rows, lat_heads, VDIM),
            preferred_element_type=jnp.float32,
        )
        return (new_max, denominator, accumulated)

    initial = (
        jnp.full((lat_heads, tok_rows), NEGATIVE, jnp.float32),
        jnp.zeros((lat_heads, tok_rows), jnp.float32),
        jnp.zeros((lat_heads, tok_rows, VDIM), jnp.float32),
    )
    pieces = (
        lax.all_gather(latent_kv, "sp", axis=0, tiled=True),
        lax.all_gather(rope_rows, "sp", axis=0, tiled=True),
    )

    def compute(current):
        piece_keys = project(pieces[0], w_key_up).astype(jnp.bfloat16)
        piece_values = project(pieces[0], w_value_up).astype(jnp.bfloat16)
        return attend(current, piece_keys, piece_values, pieces[1])

    running = lax.cond(jnp.int32(0) < row_end, compute, lambda current: current, initial)
    latent_out = jnp.transpose(running[2] / running[1][..., None], (1, 0, 2))
    latent_out = latent_out.reshape(tok_rows, lat_heads * VDIM).astype(jnp.bfloat16)
    all_window, all_latent = (
        lax.all_gather(window_out, "tp", axis=1, tiled=True),
        lax.all_gather(latent_out, "tp", axis=1, tiled=True),
    )
    column_window, column_latent = (
        lax.all_to_all(w_branch_window, "tp", split_axis=1, concat_axis=0, tiled=True),
        lax.all_to_all(w_branch_latent, "tp", split_axis=1, concat_axis=0, tiled=True),
    )
    window_branch = project(all_window, column_window)
    latent_branch = project(all_latent, column_latent)
    window_gate = jax.nn.sigmoid(project(normed, w_gate_window))
    latent_gate = jax.nn.sigmoid(project(normed, w_gate_latent))
    return (window_gate * window_branch + latent_gate * latent_branch).astype(jnp.bfloat16)


def solution(mesh):
    return jax.shard_map(
        on_device,
        mesh=mesh,
        in_specs=(
            P("sp", "tp"),
            P(),
            P(None, "tp"),
            P(None, "tp"),
            P(None, "tp"),
            P("tp"),
            P(),
            P(),
            P(),
            P(),
            P(),
            P(None, "tp"),
            P(None, "tp"),
            P(None, "tp"),
            P(None, "tp"),
            P("tp", None),
            P("tp", None),
            P(None, "tp"),
            P(None, "tp"),
        ),
        out_specs=P("sp", "tp"),
        check_vma=False,
    )
```

profile of v0, /device:TPU:0, one launch (start us, length us, event | category | flops | bytes accessed | tf_op | source)
XLA Modules:
  0.0 168.1 jit_solution(3678124389484324087)
XLA Ops:
  7.3 2.3 %copy.60 = bf16[256,2048]{0,1:T(8,128)(2,1)} copy(bf16[256,2048]{1,0:T(8,128)(2,1)} %param.37) | data formatting | bytes 2097152 | tf_op args[16]
  9.5 4.4 %all-to-all-start.1 = ((bf16[256,4,512]{0,2,1:T(8,128)(2,1)}), bf16[256,4,512]{0,2,1:T(8,128)(2,1)S(1)}, u32[]{:S(2)}, u32[]{:S(2)}) async-start(bf16[256,4,512]{0,2,1:T(8,128)(2,1)} %bitcast.96), calls=%async_computation.1 | async-start | bytes 2097152 | tf_op jit(solution)/shard_map/all_to_all | solution.py:190
  14.0 2.3 %copy.57 = bf16[256,2048]{0,1:T(8,128)(2,1)} copy(bf16[256,2048]{1,0:T(8,128)(2,1)} %param.36) | data formatting | bytes 2097152 | tf_op args[15]
  16.3 19.8 %all-to-all-done.1 = bf16[256,4,512]{0,2,1:T(8,128)(2,1)S(1)} async-done(((bf16[256,4,512]{0,2,1:T(8,128)(2,1)}), bf16[256,4,512]{0,2,1:T(8,128)(2,1)S(1)}, u32[]{:S(2)}, u32[]{:S(2)}) %all-to-all-start.1) | async-done | bytes 1048608 | tf_op jit(solution)/shard_map/all_to_all | solution.py:190
  36.1 4.2 %all-to-all-start = ((bf16[256,4,512]{0,2,1:T(8,128)(2,1)}), bf16[256,4,512]{0,2,1:T(8,128)(2,1)}, u32[]{:S(2)}, u32[]{:S(2)}) async-start(bf16[256,4,512]{0,2,1:T(8,128)(2,1)} %bitcast.97), calls=%async_computation | async-start | bytes 2097152 | tf_op jit(solution)/shard_map/all_to_all | solution.py:189
  40.7 1.3 copy.61
  42.0 12.8 %all-to-all-done = bf16[256,4,512]{0,2,1:T(8,128)(2,1)} async-done(((bf16[256,4,512]{0,2,1:T(8,128)(2,1)}), bf16[256,4,512]{0,2,1:T(8,128)(2,1)}, u32[]{:S(2)}, u32[]{:S(2)}) %all-to-all-start) | async-done | bytes 1048608 | tf_op jit(solution)/shard_map/all_to_all | solution.py:189
  54.8 2.3 %copy.58 = bf16[4,256,512]{2,1,0:T(8,128)(2,1)} copy(bf16[4,256,512]{1,2,0:T(8,128)(2,1)} %bitcast.12) | data formatting | bytes 2097152 | tf_op jit(solution)/shard_map/all_to_all | solution.py:189
  57.1 1.9 %fusion.14 = f32[384]{0:T(512)S(1)} fusion(bf16[384,2048]{1,0:T(8,128)(2,1)} %all-gather.3.cloned.1.call-done), kind=kLoop, calls=%fused_computation.22 | loop fusion | flops 2358912 | bytes 1574400 | tf_op jit(solution)/shard_map/reduce_sum | solution.py:25
  59.5 1.1 multiply_reduce_fusion.1
  61.7 2.0 %convolution_convert_fusion.6 = bf16[384,128]{0,1:T(8,128)(2,1)S(1)} fusion(bf16[384,2048]{1,0:T(8,128)(2,1)} %copy-done.2, bf16[2048,128]{1,0:T(8,128)(2,1)S(1)} %copy-done.12), kind=kOutput, calls=%fused_computation.46 | convolution fusion | flops 201375744 | bytes 2195456 | tf_op jit(solution)/shard_map/dot_general | solution.py:49
  63.8 2.0 %convolution_convert_fusion.5 = bf16[384,128]{0,1:T(8,128)(2,1)S(1)} fusion(bf16[384,2048]{1,0:T(8,128)(2,1)} %copy-done.2, bf16[2048,128]{1,0:T(8,128)(2,1)S(1)} %copy-done.13), kind=kOutput, calls=%fused_computation.45 | convolution fusion | flops 201375744 | bytes 2195456 | tf_op jit(solution)/shard_map/dot_general | solution.py:49
  66.5 5.2 %collective-permute-start = (bf16[128,256]{0,1:T(8,128)(2,1)}, bf16[128,256]{0,1:T(8,128)(2,1)}, u32[]{:S(2)}, u32[]{:S(2)}) collective-permute-start(bf16[128,256]{0,1:T(8,128)(2,1)} %pad_maximum_fusion.4), channel_id=1, source_target_pairs={{0,4},{4,8},{8,12},{12,16},{16,20},{20,24},{24,28},{1,5},{5,9},{9,... | collective-permute-start | bytes 196616 | tf_op jit(solution)/shard_map/ppermute | solution.py:19
  72.3 2.3 %convolution_convert_fusion.3 = bf16[384,256]{1,0:T(8,128)(2,1)S(1)} fusion(bf16[384,2048]{1,0:T(8,128)(2,1)} %copy-done.2, bf16[2048,256]{1,0:T(8,128)(2,1)} %param.23), kind=kOutput, calls=%fused_computation.42 | convolution fusion | flops 402751488 | bytes 2818048 | tf_op jit(solution)/shard_map/dot_general | solution.py:49
  74.9 2.1 %fusion.41 = f32[384,64]{0,1:T(8,128)S(1)} fusion(bf16[384,2048]{1,0:T(8,128)(2,1)} %copy-done.2, bf16[2048,64]{0,1:T(8,128)(2,1)S(1)} %copy-done.18), kind=kOutput, calls=%fused_computation.93 | convolution fusion | flops 100663296 | bytes 1933312 | tf_op jit(solution)/shard_map/dot_general | solution.py:49
  77.3 35.1 %all_gather.18 = bf16[3072,64]{0,1:T(8,128)(2,1)} all-gather(bf16[384,64]{0,1:T(8,128)(2,1)S(1)} %pad_maximum_fusion.5), channel_id=1, replica_groups=mesh['sp'=8,'tp'=4] {'sp'}, dimensions={0}, use_global_device_ids=true | all-gather | bytes 442368 | tf_op jit(solution)/shard_map/all_gather | solution.py:173
  112.5 2.7 %multiply_reduce_fusion = (f32[384]{0:T(512)S(1)}, f32[384,512]{1,0:T(8,128)S(1)}) fusion(bf16[384,2048]{1,0:T(8,128)(2,1)S(1)} %copy-done.3, bf16[2048,512]{1,0:T(8,128)(2,1)} %param.27), kind=kOutput, calls=%fused_computation.48 | convolution fusion | flops 805699200 | bytes 4457984 | tf_op jit(solution)/shard_map/dot_general | solution.py:49
  116.1 1.0 convolution_convert_fusion.2
  117.1 2.0 %fusion.24 = f32[384,512]{1,0:T(8,128)} fusion(bf16[384,2048]{1,0:T(8,128)(2,1)S(1)} %copy-done.3, bf16[2048,512]{1,0:T(8,128)(2,1)S(1)} %copy-done.24), kind=kOutput, calls=%fused_computation.39 | convolution fusion | flops 805896192 | bytes 4456448 | tf_op jit(solution)/shard_map/dot_general | solution.py:49
  119.1 2.0 %fusion.22 = f32[384,512]{1,0:T(8,128)} fusion(bf16[384,2048]{1,0:T(8,128)(2,1)S(1)} %copy-done.3, bf16[2048,512]{1,0:T(8,128)(2,1)S(1)} %copy-done.25), kind=kOutput, calls=%fused_computation.37 | convolution fusion | flops 805896192 | bytes 4456448 | tf_op jit(solution)/shard_map/dot_general | solution.py:49
  124.3 7.9 %all_gather.16 = bf16[384,1024]{0,1:T(8,128)(2,1)} all-gather(bf16[384,256]{0,1:T(8,128)(2,1)S(1)} %bitcast.100), channel_id=1, replica_groups=mesh['sp'=8,'tp'=4] {'tp'}, dimensions={1}, use_global_device_ids=true | all-gather | bytes 983040 | tf_op jit(solution)/shard_map/all_gather | solution.py:185
  132.2 15.7 %conditional.1 = (f32[2,384]{1,0:T(2,128)S(1)}, f32[2,384,128]{1,2,0:T(8,128)}) conditional(s32[]{:T(128)} %convert_element_type.75, () %tuple.13, (s32[]{:T(128)}, s32[384]{0:T(512)S(1)}, bf16[3072,512]{1,0:T(8,128)(2,1)}, bf16[512,256]{1,0:T(8,128)(2,1)S(1)}, bf16[384,256]{1,0:T(8,128)(2,1)}, /*index=5*/bf16[3072,64]{0,1:T(8,128)(2,1)}, ...), branch_computations={%region_5.6_spmd, %region_6.9_spmd} | conditional | flops 3146907136 | bytes 87218872 | solution.py:181
  133.1 3.4 %convolution_convert_fusion.1 = bf16[3072,256]{0,1:T(8,128)(2,1)S(1)} fusion(bf16[3072,512]{1,0:T(8,128)(2,1)} %get-tuple-element.26, bf16[512,256]{1,0:T(8,128)(2,1)S(1)} %get-tuple-element.38), kind=kOutput, calls=%fused_computation.12 | convolution fusion | flops 806092800 | bytes 4980736 | tf_op jit(solution)/shard_map/cond/branch_1_fun/dot_general | solution.py:49
  136.5 1.6 fusion.10
  138.1 2.4 %fusion.39 = (f32[2,384]{1,0:T(2,128)S(1)}, f32[2,384,3072]{1,2,0:T(8,128)S(1)}) fusion(bf16[384,2,64]{0,2,1:T(8,128)(2,1)S(1)} %copy-done.14, bf16[3072,64]{0,1:T(8,128)(2,1)S(1)} %copy-done.9, f32[2,3072,384]{2,1,0:T(8,128)S(1)} %fusion.10, pred[384,3072]{0,1:T(8,128)(4,1)S(1)} %iota_compare_fusion), kind=kOutput, calls=%fused_computation.91 | convolution fusion | flops 311426304 | bytes 20548608 | tf_op jit(solution)/shard_map/cond/branch_1_fun/qhr,kr->hqk/dot_general | solution.py:148
  140.5 1.0 convolution_convert_fusion
  141.6 3.1 %fusion.4 = f32[2,384,128]{1,2,0:T(8,128)} fusion(bf16[3072,2,128]{0,2,1:T(8,128)(2,1)S(1)} %bitcast.93, f32[2,384,3072]{1,2,0:T(8,128)S(1)} %get-tuple-element.42, f32[2,384]{1,0:T(2,128)S(1)} %broadcast_maximum_fusion, pred[384,3072]{0,1:T(8,128)(4,1)S(1)} %iota_compare_fusion), kind=kOutput, calls=%fused_computation.6 | convolution fusion | flops 611057664 | bytes 12585984 | tf_op jit(solution)/shard_map/cond | solution.py:181
  144.7 3.2 %fusion.3 = f32[2,384]{1,0:T(2,128)S(1)} fusion(f32[2,384,3072]{1,2,0:T(8,128)S(1)} %get-tuple-element.42, f32[2,384]{1,0:T(2,128)S(1)} %broadcast_maximum_fusion, pred[384,3072]{0,1:T(8,128)(4,1)} %copy-done.4), kind=kLoop, calls=%fused_computation.5 | loop fusion | flops 7077120 | bytes 10622976 | tf_op jit(solution)/shard_map/cond/branch_1_fun/reduce_sum | solution.py:157
  147.9 1.1 divide_convert_fusion.2
  149.0 9.0 %all_gather.19 = bf16[384,1024]{0,1:T(8,128)(2,1)S(1)} all-gather(bf16[384,256]{0,1:T(8,128)(2,1)S(1)} %bitcast.102), channel_id=1, replica_groups=mesh['sp'=8,'tp'=4] {'tp'}, dimensions={1}, use_global_device_ids=true | all-gather | bytes 983040 | tf_op jit(solution)/shard_map/all_gather | solution.py:186
  158.0 1.9 %convolution_multiply_fusion = f32[384,512]{1,0:T(8,128)S(1)} fusion(f32[384,512]{1,0:T(8,128)} %fusion.24, bf16[384,1024]{0,1:T(8,128)(2,1)S(1)} %all_gather.19, bf16[1024,512]{1,0:T(8,128)(2,1)S(1)} %bitcast.94), kind=kOutput, calls=%fused_computation.28 | convolution fusion | flops 402849792 | bytes 3407872 | tf_op jit(solution)/shard_map/dot_general | solution.py:49
  159.9 1.4 fusion.25
  (101 shorter events, 9.6 us)
Async XLA Ops:
  6.5 53.0 %copy-start = (bf16[2048,512]{1,0:T(8,128)(2,1)S(1)}, bf16[2048,512]{1,0:T(8,128)(2,1)}, u32[]{:S(2)}) copy-start(bf16[2048,512]{1,0:T(8,128)(2,1)} %param.28) | copy-start | bytes 6291460
  6.5 50.6 %all-gather.3.cloned.1.call-start = ((), (), s32[]{:S(2)}) async-start(), calls=%async_computation.2 | async-start | bytes 1966080 | tf_op jit(solution)/shard_map/all_gather | solution.py:112
  9.5 4.4 %copy-start.26 = (f32[4]{0:T(128)S(1)}, f32[4]{0:T(128)}, u32[]{:S(2)}) copy-start(f32[4]{0:T(128)} %param.26) | copy-start | bytes 52
  9.5 26.6 %all-to-all-start.1 = ((bf16[256,4,512]{0,2,1:T(8,128)(2,1)}), bf16[256,4,512]{0,2,1:T(8,128)(2,1)S(1)}, u32[]{:S(2)}, u32[]{:S(2)}) async-start(bf16[256,4,512]{0,2,1:T(8,128)(2,1)} %bitcast.96), calls=%async_computation.1 | async-start | bytes 2097152 | tf_op jit(solution)/shard_map/all_to_all | solution.py:190
  36.1 18.7 %all-to-all-start = ((bf16[256,4,512]{0,2,1:T(8,128)(2,1)}), bf16[256,4,512]{0,2,1:T(8,128)(2,1)}, u32[]{:S(2)}, u32[]{:S(2)}) async-start(bf16[256,4,512]{0,2,1:T(8,128)(2,1)} %bitcast.97), calls=%async_computation | async-start | bytes 2097152 | tf_op jit(solution)/shard_map/all_to_all | solution.py:189
  40.3 91.8 %all-gather.5.cloned.1.call-start = ((), (), s32[]{:S(2)}) async-start(), calls=%async_computation.3 | async-start | bytes 3538944 | tf_op jit(solution)/shard_map/all_gather | solution.py:172
  54.8 4.2 %copy-start.21 = (f32[2048]{0:T(1024)S(1)}, f32[2048]{0:T(1024)}, u32[]{:S(2)}) copy-start(f32[2048]{0:T(1024)} %param.22) | copy-start | bytes 24580
  57.1 1.9 %copy-start.5 = (bf16[384,2048]{1,0:T(8,128)(2,1)S(1)}, bf16[384,2048]{1,0:T(8,128)(2,1)}, u32[]{:S(2)}) copy-start(bf16[384,2048]{1,0:T(8,128)(2,1)} %all-gather.3.cloned.1.call-done) | copy-start | bytes 4718596
  59.5 1.2 copy-start.2
  59.5 1.2 copy-start.23
  60.7 1.0 copy-start.12
  61.6 2.2 %copy-start.13 = (bf16[2048,128]{1,0:T(8,128)(2,1)S(1)}, bf16[2048,128]{1,0:T(8,128)(2,1)}, u32[]{:S(2)}) copy-start(bf16[2048,128]{1,0:T(8,128)(2,1)} %param.25) | copy-start | bytes 1572868
  66.5 55.2 %collective-permute-start = (bf16[128,256]{0,1:T(8,128)(2,1)}, bf16[128,256]{0,1:T(8,128)(2,1)}, u32[]{:S(2)}, u32[]{:S(2)}) collective-permute-start(bf16[128,256]{0,1:T(8,128)(2,1)} %pad_maximum_fusion.4), channel_id=1, source_target_pairs={{0,4},{4,8},{8,12},{12,16},{16,20},{20,24},{24,28},{1,5},{5,9},{9,... | collective-permute-start | bytes 196616 | tf_op jit(solution)/shard_map/ppermute | solution.py:19
  72.3 2.6 %copy-start.18 = (bf16[2048,64]{0,1:T(8,128)(2,1)S(1)}, bf16[2048,64]{0,1:T(8,128)(2,1)}, u32[]{:S(2)}) copy-start(bf16[2048,64]{0,1:T(8,128)(2,1)} %param.29) | copy-start | bytes 786436
  74.9 37.6 %copy-start.3 = (bf16[384,2048]{1,0:T(8,128)(2,1)S(1)}, bf16[384,2048]{1,0:T(8,128)(2,1)}, u32[]{:S(2)}) copy-start(bf16[384,2048]{1,0:T(8,128)(2,1)} %copy-done.2) | copy-start | bytes 4718596
  112.4 2.7 %copy-start.19 = (bf16[512,128]{1,0:T(8,128)(2,1)S(1)}, bf16[512,128]{1,0:T(8,128)(2,1)}, u32[]{:S(2)}) copy-start(bf16[512,128]{1,0:T(8,128)(2,1)} %param.33) | copy-start | bytes 393220
  112.4 2.7 %copy-start.22 = (f32[512]{0:T(512)S(1)}, f32[512]{0:T(512)}, u32[]{:S(2)}) copy-start(f32[512]{0:T(512)} %param.30) | copy-start | bytes 6148
  115.1 1.0 copy-start.15
  115.1 1.9 %copy-start.24 = (bf16[2048,512]{1,0:T(8,128)(2,1)S(1)}, bf16[2048,512]{1,0:T(8,128)(2,1)}, u32[]{:S(2)}) copy-start(bf16[2048,512]{1,0:T(8,128)(2,1)} %param.39) | copy-start | bytes 6291460
  117.1 2.0 %copy-start.25 = (bf16[2048,512]{1,0:T(8,128)(2,1)S(1)}, bf16[2048,512]{1,0:T(8,128)(2,1)}, u32[]{:S(2)}) copy-start(bf16[2048,512]{1,0:T(8,128)(2,1)} %param.38) | copy-start | bytes 6291460
  121.0 1.6 copy-start.20
  124.0 8.1 %copy-start.16 = (bf16[512,256]{1,0:T(8,128)(2,1)S(1)}, bf16[512,256]{1,0:T(8,128)(2,1)}, u32[]{:S(2)}) copy-start(bf16[512,256]{1,0:T(8,128)(2,1)} %param.34) | copy-start | bytes 786436
  133.1 8.5 %copy-start.4 = (pred[384,3072]{0,1:T(8,128)(4,1)}, pred[384,3072]{0,1:T(8,128)(4,1)S(1)}, u32[]{:S(2)}) copy-start(pred[384,3072]{0,1:T(8,128)(4,1)S(1)} %iota_compare_fusion) | copy-start | bytes 3538948 | tf_op jit(solution)/shard_map/cond
  133.1 3.4 %copy-start.11 = (bf16[384,256]{1,0:T(8,128)(2,1)S(1)}, bf16[384,256]{1,0:T(8,128)(2,1)}, u32[]{:S(2)}) copy-start(bf16[384,256]{1,0:T(8,128)(2,1)} %get-tuple-element.28) | copy-start | bytes 589828 | tf_op jit(solution)/shard_map/cond
  136.5 1.6 copy-start.9
  136.5 1.6 copy-start.14
  138.1 2.5 %copy-start.1 = (bf16[3072,512]{1,0:T(8,128)(2,1)S(1)}, bf16[3072,512]{1,0:T(8,128)(2,1)}, u32[]{:S(2)}) copy-start(bf16[3072,512]{1,0:T(8,128)(2,1)} %get-tuple-element.26) | copy-start | bytes 9437188 | tf_op jit(solution)/shard_map/cond
  138.1 2.5 %copy-start.17 = (bf16[512,256]{1,0:T(8,128)(2,1)S(1)}, bf16[512,256]{1,0:T(8,128)(2,1)}, u32[]{:S(2)}) copy-start(bf16[512,256]{1,0:T(8,128)(2,1)} %get-tuple-element.39) | copy-start | bytes 786436 | tf_op jit(solution)/shard_map/cond
  147.9 10.1 %copy-start.6 = (bf16[4,256,512]{2,1,0:T(8,128)(2,1)S(1)}, bf16[4,256,512]{2,1,0:T(8,128)(2,1)}, u32[]{:S(2)}) copy-start(bf16[4,256,512]{2,1,0:T(8,128)(2,1)} %copy.61) | copy-start | bytes 3145732
  158.0 1.9 %copy-start.7 = (bf16[4,256,512]{2,1,0:T(8,128)(2,1)S(1)}, bf16[4,256,512]{2,1,0:T(8,128)(2,1)}, u32[]{:S(2)}) copy-start(bf16[4,256,512]{2,1,0:T(8,128)(2,1)} %copy.58) | copy-start | bytes 3145732
  158.0 1.9 %copy-start.8 = (bf16[384,1024]{0,1:T(8,128)(2,1)S(1)}, bf16[384,1024]{0,1:T(8,128)(2,1)}, u32[]{:S(2)}) copy-start(bf16[384,1024]{0,1:T(8,128)(2,1)} %all_gather.16) | copy-start | bytes 2359300
  158.0 1.9 %copy-start.10 = (f32[384,512]{1,0:T(8,128)S(1)}, f32[384,512]{1,0:T(8,128)}, u32[]{:S(2)}) copy-start(f32[384,512]{1,0:T(8,128)} %fusion.22) | copy-start | bytes 2359300
Sparse Core Ops, SparseCore 0:
  8.9 29.3 all-gather.2
  61.7 65.5 all-gather.4
where the time goes:
time: 169 us; the launch traced here: 168 us
  blocking collectives  52 us (31%)
  waiting for transfers between devices  33.3 us (20%)
  matrix products  33.2 us (20%)
  starting transfers between devices  13.9 us (8%)
  between operations  13.7 us (8%)
  other arithmetic  11.6 us (7%)
  local copies, waits for them, and re-layouts  10.3 us (6%)
    all_gather x1, blocking collectives, on_device(): lax.all_gather(rope_rows, 'sp', axis=0, tiled=True)  35.1 us
    dot_general x14, matrix products, project(): return jnp.dot(left, right, preferred_element_type=jnp.float32)  25.1 us
    all_to_all x1, waiting for transfers between devices, on_device(): lax.all_to_all(w_branch_latent, 'tp', split_axis=1, concat_axis=0, tiled=...  19.8 us
    all_to_all x1, waiting for transfers between devices, on_device(): lax.all_to_all(w_branch_window, 'tp', split_axis=1, concat_axis=0, tiled=...  12.8 us
    all_gather x1, blocking collectives, on_device(): lax.all_gather(latent_out, 'tp', axis=1, tiled=True)  8.98 us
    all_gather x1, blocking collectives, on_device(): lax.all_gather(window_out, 'tp', axis=1, tiled=True)  7.89 us
    unnamed x45, local copies, waits for them, and re-layouts  5.36 us
    ppermute x1, starting transfers between devices, from_behind(): return lax.ppermute(shard, axis, pairs)  5.23 us
  transfers between devices with their start and end apart: 5, of which 2 were waited for; matrix products, arithmetic and copies ran while one was open for 18% of the time, Pallas kernels for 0%

commit v1 on v0

--- a/solution.py
+++ b/solution.py
@@ -11,6 +11,15 @@
 EPS = 1e-06
 THETA = 10000.0
 NEGATIVE = -1e30
+return_all_lines_for = lambda block_here, k_dim, in_dim: jnp.concatenate(
+    jax.lax.all_to_all(
+        jnp.stack(jnp.split(block_here, jax.lax.axis_size("tp"), axis=k_dim)),
+        axis_name="tp",
+        split_axis=0,
+        concat_axis=0,
+    ),
+    axis=in_dim,
+)
 
 
 def from_behind(shard, axis, by):
@@ -186,7 +195,7 @@
         lax.all_gather(latent_out, "tp", axis=1, tiled=True),
     )
     column_window, column_latent = (
-        lax.all_to_all(w_branch_window, "tp", split_axis=1, concat_axis=0, tiled=True),
+        return_all_lines_for(w_branch_window, 1, in_dim=0),
         lax.all_to_all(w_branch_latent, "tp", split_axis=1, concat_axis=0, tiled=True),
     )
     window_branch = project(all_window, column_window)

time: 169 us -> 157 us (0.929)
  waiting for transfers between devices: 33.3 us -> 20.1 us
  local copies, waits for them, and re-layouts: 10.3 us -> 6.99 us
  matrix products: 33.2 us -> 35.8 us
    all_to_all x1, waiting for transfers between devices: 12.8 us -> 0.01 us  [jax.lax.all_to_all(jnp.stack(jnp.split(block_here, jax.lax.axis_size('tp'...]
    dot_general x14, matrix products: 25.1 us -> 27.7 us  [project(): return jnp.dot(left, right, preferred_element_type=jnp.float32)]
    all_to_all x1 -> x0, local copies, waits for them, and re-layouts: 2.28 us -> none  [on_device(): lax.all_to_all(w_branch_window, 'tp', split_axis=1, concat_axis=0, tiled=...]
    unnamed x45 -> x40, local copies, waits for them, and re-layouts: 5.36 us -> 3.08 us
  transfers between devices with their start and end apart: 5 -> 5, of which waited for: 2 -> 1; matrix products, arithmetic and copies ran while one was open for 18% -> 33% of each run, Pallas kernels for 0% -> 0%
where the time goes in v1:
time: 157 us; the launch traced here: 156 us
  blocking collectives  52.9 us (34%)
  matrix products  35.8 us (23%)
  waiting for transfers between devices  20.1 us (13%)
  starting transfers between devices  13.9 us (9%)
  between operations  13.7 us (9%)
  other arithmetic  12.7 us (8%)
  local copies, waits for them, and re-layouts  6.99 us (4%)
    all_gather x1, blocking collectives, on_device(): lax.all_gather(rope_rows, 'sp', axis=0, tiled=True)  34.6 us
    dot_general x14, matrix products, project(): return jnp.dot(left, right, preferred_element_type=jnp.float32)  27.7 us
    all_to_all x1, waiting for transfers between devices, on_device(): lax.all_to_all(w_branch_latent, 'tp', split_axis=1, concat_axis=0, tiled=...  19.4 us
    all_gather x1, blocking collectives, on_device(): lax.all_gather(window_out, 'tp', axis=1, tiled=True)  9.54 us
    all_gather x1, blocking collectives, on_device(): lax.all_gather(latent_out, 'tp', axis=1, tiled=True)  8.72 us
    ppermute x1, starting transfers between devices, from_behind(): return lax.ppermute(shard, axis, pairs)  5.23 us
    all_to_all x1, starting transfers between devices, on_device(): lax.all_to_all(w_branch_latent, 'tp', split_axis=1, concat_axis=0, tiled=...  4.4 us
    all_to_all x1, starting transfers between devices, jax.lax.all_to_all(jnp.stack(jnp.split(block_here, jax.lax.axis_size('tp'...  4.24 us
  transfers between devices with their start and end apart: 5, of which 1 were waited for; matrix products, arithmetic and copies ran while one was open for 33% of the time, Pallas kernels for 0%

profile of v1, /device:TPU:0, one launch (start us, length us, event | category | flops | bytes accessed | tf_op | source)
XLA Modules:
  0.0 156.2 jit_solution(14720153579535562329)
XLA Ops:
  7.3 2.3 %copy.58 = bf16[256,2048]{0,1:T(8,128)(2,1)} copy(bf16[256,2048]{1,0:T(8,128)(2,1)} %param.37) | data formatting | bytes 2097152 | tf_op args[16]
  9.5 4.4 %all-to-all-start.1 = ((bf16[256,4,512]{0,2,1:T(8,128)(2,1)}), bf16[256,4,512]{0,2,1:T(8,128)(2,1)S(1)}, u32[]{:S(2)}, u32[]{:S(2)}) async-start(bf16[256,4,512]{0,2,1:T(8,128)(2,1)} %bitcast.102), calls=%async_computation.1 | async-start | bytes 2097152 | tf_op jit(solution)/shard_map/all_to_all | solution.py:199
  14.0 1.3 slice_bitcast_fusion.3
  15.3 1.1 pad_maximum_fusion
  16.7 19.4 %all-to-all-done.1 = bf16[256,4,512]{0,2,1:T(8,128)(2,1)S(1)} async-done(((bf16[256,4,512]{0,2,1:T(8,128)(2,1)}), bf16[256,4,512]{0,2,1:T(8,128)(2,1)S(1)}, u32[]{:S(2)}, u32[]{:S(2)}) %all-to-all-start.1) | async-done | bytes 1048608 | tf_op jit(solution)/shard_map/all_to_all | solution.py:199
  36.1 4.2 %all-to-all-start = ((bf16[4,256,512]{2,1,0:T(8,128)(2,1)}), bf16[4,256,512]{2,1,0:T(8,128)(2,1)}, u32[]{:S(2)}, u32[]{:S(2)}) async-start(bf16[4,256,512]{2,1,0:T(8,128)(2,1)} %pad_maximum_fusion), calls=%async_computation | async-start | bytes 2097152 | tf_op jit(solution)/shard_map/all_to_all | solution.py:15
  40.4 1.3 copy.59
  41.7 1.9 %fusion.14 = f32[384]{0:T(512)S(1)} fusion(bf16[384,2048]{1,0:T(8,128)(2,1)} %all-gather.3.cloned.1.call-done), kind=kLoop, calls=%fused_computation.22 | loop fusion | flops 2358912 | bytes 1574400 | tf_op jit(solution)/shard_map/reduce_sum | solution.py:34
  44.1 1.1 multiply_reduce_fusion.1
  46.3 2.0 %convolution_convert_fusion.6 = bf16[384,128]{0,1:T(8,128)(2,1)S(1)} fusion(bf16[384,2048]{1,0:T(8,128)(2,1)} %copy-done.2, bf16[2048,128]{1,0:T(8,128)(2,1)S(1)} %copy-done.10), kind=kOutput, calls=%fused_computation.46 | convolution fusion | flops 201375744 | bytes 2195456 | tf_op jit(solution)/shard_map/dot_general | solution.py:58
  48.4 2.0 %convolution_convert_fusion.5 = bf16[384,128]{0,1:T(8,128)(2,1)S(1)} fusion(bf16[384,2048]{1,0:T(8,128)(2,1)} %copy-done.2, bf16[2048,128]{1,0:T(8,128)(2,1)S(1)} %copy-done.11), kind=kOutput, calls=%fused_computation.45 | convolution fusion | flops 201375744 | bytes 2195456 | tf_op jit(solution)/shard_map/dot_general | solution.py:58
  51.1 5.2 %collective-permute-start = (bf16[128,256]{0,1:T(8,128)(2,1)}, bf16[128,256]{0,1:T(8,128)(2,1)}, u32[]{:S(2)}, u32[]{:S(2)}) collective-permute-start(bf16[128,256]{0,1:T(8,128)(2,1)} %pad_maximum_fusion.5), channel_id=1, source_target_pairs={{0,4},{4,8},{8,12},{12,16},{16,20},{20,24},{24,28},{1,5},{5,9},{9,... | collective-permute-start | bytes 196616 | tf_op jit(solution)/shard_map/ppermute | solution.py:28
  56.9 2.4 %convolution_convert_fusion.3 = bf16[384,256]{1,0:T(8,128)(2,1)S(1)} fusion(bf16[384,2048]{1,0:T(8,128)(2,1)} %copy-done.2, bf16[2048,256]{1,0:T(8,128)(2,1)} %param.23), kind=kOutput, calls=%fused_computation.42 | convolution fusion | flops 402751488 | bytes 2818048 | tf_op jit(solution)/shard_map/dot_general | solution.py:58
  59.6 2.1 %fusion.41 = f32[384,64]{0,1:T(8,128)S(1)} fusion(bf16[384,2048]{1,0:T(8,128)(2,1)} %copy-done.2, bf16[2048,64]{0,1:T(8,128)(2,1)S(1)} %copy-done.16), kind=kOutput, calls=%fused_computation.98 | convolution fusion | flops 100663296 | bytes 1933312 | tf_op jit(solution)/shard_map/dot_general | solution.py:58
  62.0 34.6 %all_gather.18 = bf16[3072,64]{0,1:T(8,128)(2,1)} all-gather(bf16[384,64]{0,1:T(8,128)(2,1)S(1)} %pad_maximum_fusion.6), channel_id=1, replica_groups=mesh['sp'=8,'tp'=4] {'sp'}, dimensions={0}, use_global_device_ids=true | all-gather | bytes 442368 | tf_op jit(solution)/shard_map/all_gather | solution.py:182
  96.7 2.7 %multiply_reduce_fusion = (f32[384]{0:T(512)S(1)}, f32[384,512]{1,0:T(8,128)S(1)}) fusion(bf16[384,2048]{1,0:T(8,128)(2,1)S(1)} %copy-done.3, bf16[2048,512]{1,0:T(8,128)(2,1)} %param.27), kind=kOutput, calls=%fused_computation.49 | convolution fusion | flops 805699200 | bytes 4457984 | tf_op jit(solution)/shard_map/dot_general | solution.py:58
  100.3 1.0 convolution_convert_fusion.2
  101.3 2.0 %fusion.24 = f32[384,512]{1,0:T(8,128)} fusion(bf16[384,2048]{1,0:T(8,128)(2,1)S(1)} %copy-done.3, bf16[2048,512]{1,0:T(8,128)(2,1)S(1)} %copy-done.22), kind=kOutput, calls=%fused_computation.39 | convolution fusion | flops 805896192 | bytes 4456448 | tf_op jit(solution)/shard_map/dot_general | solution.py:58
  103.3 2.0 %fusion.22 = f32[384,512]{1,0:T(8,128)} fusion(bf16[384,2048]{1,0:T(8,128)(2,1)S(1)} %copy-done.3, bf16[2048,512]{1,0:T(8,128)(2,1)S(1)} %copy-done.23), kind=kOutput, calls=%fused_computation.37 | convolution fusion | flops 805896192 | bytes 4456448 | tf_op jit(solution)/shard_map/dot_general | solution.py:58
  108.5 9.5 %all_gather.16 = bf16[384,1024]{0,1:T(8,128)(2,1)} all-gather(bf16[384,256]{0,1:T(8,128)(2,1)S(1)} %bitcast.104), channel_id=1, replica_groups=mesh['sp'=8,'tp'=4] {'tp'}, dimensions={1}, use_global_device_ids=true | all-gather | bytes 983040 | tf_op jit(solution)/shard_map/all_gather | solution.py:194
  118.0 15.7 %conditional.1 = (f32[2,384]{1,0:T(2,128)S(1)}, f32[2,384,128]{1,2,0:T(8,128)}) conditional(s32[]{:T(128)} %convert_element_type.75, () %tuple.13, (s32[]{:T(128)}, s32[384]{0:T(512)S(1)}, bf16[3072,512]{1,0:T(8,128)(2,1)}, bf16[512,256]{1,0:T(8,128)(2,1)S(1)}, bf16[384,256]{1,0:T(8,128)(2,1)}, /*index=5*/bf16[3072,64]{0,1:T(8,128)(2,1)}, ...), branch_computations={%region_5.6_spmd, %region_6.9_spmd} | conditional | flops 3146907136 | bytes 87218872 | solution.py:190
  118.1 0.9 iota_compare_fusion
  119.0 3.4 %convolution_convert_fusion.1 = bf16[3072,256]{0,1:T(8,128)(2,1)S(1)} fusion(bf16[3072,512]{1,0:T(8,128)(2,1)} %get-tuple-element.26, bf16[512,256]{1,0:T(8,128)(2,1)S(1)} %get-tuple-element.38), kind=kOutput, calls=%fused_computation.12 | convolution fusion | flops 806092800 | bytes 4980736 | tf_op jit(solution)/shard_map/cond/branch_1_fun/dot_general | solution.py:58
  122.4 1.6 %fusion.10 = f32[2,3072,384]{2,1,0:T(8,128)S(1)} fusion(bf16[3072,2,128]{0,2,1:T(8,128)(2,1)S(1)} %bitcast.98, bf16[384,256]{1,0:T(8,128)(2,1)S(1)} %copy-done.9), kind=kOutput, calls=%fused_computation.14 | convolution fusion | flops 603979776 | bytes 11206656 | tf_op jit(solution)/shard_map/cond/branch_1_fun/qhd,khd->hqk/dot_general | solution.py:151
  124.0 2.4 %fusion.39 = (f32[2,384]{1,0:T(2,128)S(1)}, f32[2,384,3072]{1,2,0:T(8,128)S(1)}) fusion(bf16[384,2,64]{0,2,1:T(8,128)(2,1)S(1)} %copy-done.12, bf16[3072,64]{0,1:T(8,128)(2,1)S(1)} %copy-done.8, f32[2,3072,384]{2,1,0:T(8,128)S(1)} %fusion.10, pred[384,3072]{0,1:T(8,128)(4,1)S(1)} %iota_compare_fusion), kind=kOutput, calls=%fused_computation.96 | convolution fusion | flops 311426304 | bytes 20548608 | tf_op jit(solution)/shard_map/cond/branch_1_fun/qhr,kr->hqk/dot_general | solution.py:157
  126.4 1.0 convolution_convert_fusion
  127.5 3.1 %fusion.4 = f32[2,384,128]{1,2,0:T(8,128)} fusion(bf16[3072,2,128]{0,2,1:T(8,128)(2,1)S(1)} %bitcast.99, f32[2,384,3072]{1,2,0:T(8,128)S(1)} %get-tuple-element.42, f32[2,384]{1,0:T(2,128)S(1)} %broadcast_maximum_fusion, pred[384,3072]{0,1:T(8,128)(4,1)S(1)} %iota_compare_fusion), kind=kOutput, calls=%fused_computation.6 | convolution fusion | flops 611057664 | bytes 12585984 | tf_op jit(solution)/shard_map/cond | solution.py:190
  130.6 3.2 %fusion.3 = f32[2,384]{1,0:T(2,128)S(1)} fusion(f32[2,384,3072]{1,2,0:T(8,128)S(1)} %get-tuple-element.42, f32[2,384]{1,0:T(2,128)S(1)} %broadcast_maximum_fusion, pred[384,3072]{0,1:T(8,128)(4,1)} %copy-done.4), kind=kLoop, calls=%fused_computation.5 | loop fusion | flops 7077120 | bytes 10622976 | tf_op jit(solution)/shard_map/cond/branch_1_fun/reduce_sum | solution.py:166
  133.8 1.1 divide_convert_fusion.2
  134.9 8.7 %all_gather.19 = bf16[384,1024]{0,1:T(8,128)(2,1)S(1)} all-gather(bf16[384,256]{0,1:T(8,128)(2,1)S(1)} %bitcast.106), channel_id=1, replica_groups=mesh['sp'=8,'tp'=4] {'tp'}, dimensions={1}, use_global_device_ids=true | all-gather | bytes 983040 | tf_op jit(solution)/shard_map/all_gather | solution.py:195
  143.7 2.7 %convolution_multiply_fusion = f32[384,512]{1,0:T(8,128)} fusion(f32[384,512]{1,0:T(8,128)} %fusion.24, bf16[384,1024]{0,1:T(8,128)(2,1)S(1)} %all_gather.19, bf16[1024,512]{1,0:T(8,128)(2,1)S(1)} %bitcast.100), kind=kOutput, calls=%fused_computation.28 | convolution fusion | flops 402849792 | bytes 3407872 | tf_op jit(solution)/shard_map/dot_general | solution.py:58
  146.4 3.0 %fusion.25 = bf16[384,512]{1,0:T(8,128)(2,1)} fusion(f32[384,512]{1,0:T(8,128)} %convolution_multiply_fusion, f32[384,512]{1,0:T(8,128)} %fusion.22, bf16[384,1024]{0,1:T(8,128)(2,1)S(1)} %copy-done.7, bf16[1024,512]{1,0:T(8,128)(2,1)} %bitcast.15), kind=kOutput, calls=%fused_computation.40 | convolution fusion | flops 403243008 | bytes 3801088 | tf_op jit(solution)/shard_map/dot_general | solution.py:58
  (97 shorter events, 8.7 us)
Async XLA Ops:
  6.5 37.6 %copy-start = (bf16[2048,512]{1,0:T(8,128)(2,1)S(1)}, bf16[2048,512]{1,0:T(8,128)(2,1)}, u32[]{:S(2)}) copy-start(bf16[2048,512]{1,0:T(8,128)(2,1)} %param.28) | copy-start | bytes 6291460
  6.5 35.2 %all-gather.3.cloned.1.call-start = ((), (), s32[]{:S(2)}) async-start(), calls=%async_computation.2 | async-start | bytes 1966080 | tf_op jit(solution)/shard_map/all_gather | solution.py:121
  9.5 4.4 %copy-start.24 = (f32[4]{0:T(128)S(1)}, f32[4]{0:T(128)}, u32[]{:S(2)}) copy-start(f32[4]{0:T(128)} %param.26) | copy-start | bytes 52
  9.5 26.6 %all-to-all-start.1 = ((bf16[256,4,512]{0,2,1:T(8,128)(2,1)}), bf16[256,4,512]{0,2,1:T(8,128)(2,1)S(1)}, u32[]{:S(2)}, u32[]{:S(2)}) async-start(bf16[256,4,512]{0,2,1:T(8,128)(2,1)} %bitcast.102), calls=%async_computation.1 | async-start | bytes 2097152 | tf_op jit(solution)/shard_map/all_to_all | solution.py:199
  36.1 110.3 %all-to-all-start = ((bf16[4,256,512]{2,1,0:T(8,128)(2,1)}), bf16[4,256,512]{2,1,0:T(8,128)(2,1)}, u32[]{:S(2)}, u32[]{:S(2)}) async-start(bf16[4,256,512]{2,1,0:T(8,128)(2,1)} %pad_maximum_fusion), calls=%async_computation | async-start | bytes 2097152 | tf_op jit(solution)/shard_map/all_to_all | solution.py:15
  40.3 77.7 %all-gather.5.cloned.1.call-start = ((), (), s32[]{:S(2)}) async-start(), calls=%async_computation.3 | async-start | bytes 3538944 | tf_op jit(solution)/shard_map/all_gather | solution.py:181
  40.4 3.3 %copy-start.19 = (f32[2048]{0:T(1024)S(1)}, f32[2048]{0:T(1024)}, u32[]{:S(2)}) copy-start(f32[2048]{0:T(1024)} %param.22) | copy-start | bytes 24580
  41.7 1.9 %copy-start.5 = (bf16[384,2048]{1,0:T(8,128)(2,1)S(1)}, bf16[384,2048]{1,0:T(8,128)(2,1)}, u32[]{:S(2)}) copy-start(bf16[384,2048]{1,0:T(8,128)(2,1)} %all-gather.3.cloned.1.call-done) | copy-start | bytes 4718596
  44.1 1.2 copy-start.2
  44.1 1.2 copy-start.21
  45.3 1.0 copy-start.10
  46.2 2.2 %copy-start.11 = (bf16[2048,128]{1,0:T(8,128)(2,1)S(1)}, bf16[2048,128]{1,0:T(8,128)(2,1)}, u32[]{:S(2)}) copy-start(bf16[2048,128]{1,0:T(8,128)(2,1)} %param.25) | copy-start | bytes 1572868
  51.1 54.9 %collective-permute-start = (bf16[128,256]{0,1:T(8,128)(2,1)}, bf16[128,256]{0,1:T(8,128)(2,1)}, u32[]{:S(2)}, u32[]{:S(2)}) collective-permute-start(bf16[128,256]{0,1:T(8,128)(2,1)} %pad_maximum_fusion.5), channel_id=1, source_target_pairs={{0,4},{4,8},{8,12},{12,16},{16,20},{20,24},{24,28},{1,5},{5,9},{9,... | collective-permute-start | bytes 196616 | tf_op jit(solution)/shard_map/ppermute | solution.py:28
  56.9 2.7 %copy-start.16 = (bf16[2048,64]{0,1:T(8,128)(2,1)S(1)}, bf16[2048,64]{0,1:T(8,128)(2,1)}, u32[]{:S(2)}) copy-start(bf16[2048,64]{0,1:T(8,128)(2,1)} %param.29) | copy-start | bytes 786436
  59.6 37.1 %copy-start.3 = (bf16[384,2048]{1,0:T(8,128)(2,1)S(1)}, bf16[384,2048]{1,0:T(8,128)(2,1)}, u32[]{:S(2)}) copy-start(bf16[384,2048]{1,0:T(8,128)(2,1)} %copy-done.2) | copy-start | bytes 4718596
  96.7 2.7 %copy-start.17 = (bf16[512,128]{1,0:T(8,128)(2,1)S(1)}, bf16[512,128]{1,0:T(8,128)(2,1)}, u32[]{:S(2)}) copy-start(bf16[512,128]{1,0:T(8,128)(2,1)} %param.33) | copy-start | bytes 393220
  96.7 2.7 %copy-start.20 = (f32[512]{0:T(512)S(1)}, f32[512]{0:T(512)}, u32[]{:S(2)}) copy-start(f32[512]{0:T(512)} %param.30) | copy-start | bytes 6148
  99.4 1.0 copy-start.13
  99.4 1.9 %copy-start.22 = (bf16[2048,512]{1,0:T(8,128)(2,1)S(1)}, bf16[2048,512]{1,0:T(8,128)(2,1)}, u32[]{:S(2)}) copy-start(bf16[2048,512]{1,0:T(8,128)(2,1)} %param.39) | copy-start | bytes 6291460
  101.3 2.0 %copy-start.23 = (bf16[2048,512]{1,0:T(8,128)(2,1)S(1)}, bf16[2048,512]{1,0:T(8,128)(2,1)}, u32[]{:S(2)}) copy-start(bf16[2048,512]{1,0:T(8,128)(2,1)} %param.38) | copy-start | bytes 6291460
  105.3 1.6 %copy-start.18 = (bf16[3,128,2,64]{1,3,2,0:T(8,128)(2,1)S(1)}, bf16[3,128,2,64]{1,3,2,0:T(8,128)(2,1)}, u32[]{:S(2)}) copy-start(bf16[3,128,2,64]{1,3,2,0:T(8,128)(2,1)} %copy.52) | copy-start | bytes 294916
  108.3 9.8 %copy-start.14 = (bf16[512,256]{1,0:T(8,128)(2,1)S(1)}, bf16[512,256]{1,0:T(8,128)(2,1)}, u32[]{:S(2)}) copy-start(bf16[512,256]{1,0:T(8,128)(2,1)} %param.34) | copy-start | bytes 786436
  119.0 8.5 %copy-start.4 = (pred[384,3072]{0,1:T(8,128)(4,1)}, pred[384,3072]{0,1:T(8,128)(4,1)S(1)}, u32[]{:S(2)}) copy-start(pred[384,3072]{0,1:T(8,128)(4,1)S(1)} %iota_compare_fusion) | copy-start | bytes 3538948 | tf_op jit(solution)/shard_map/cond
  119.0 3.4 %copy-start.9 = (bf16[384,256]{1,0:T(8,128)(2,1)S(1)}, bf16[384,256]{1,0:T(8,128)(2,1)}, u32[]{:S(2)}) copy-start(bf16[384,256]{1,0:T(8,128)(2,1)} %get-tuple-element.28) | copy-start | bytes 589828 | tf_op jit(solution)/shard_map/cond
  122.3 1.6 %copy-start.8 = (bf16[3072,64]{0,1:T(8,128)(2,1)S(1)}, bf16[3072,64]{0,1:T(8,128)(2,1)}, u32[]{:S(2)}) copy-start(bf16[3072,64]{0,1:T(8,128)(2,1)} %get-tuple-element.29) | copy-start | bytes 1179652 | tf_op jit(solution)/shard_map/cond
  122.4 1.6 %copy-start.12 = (bf16[384,2,64]{0,2,1:T(8,128)(2,1)S(1)}, bf16[384,2,64]{0,2,1:T(8,128)(2,1)}, u32[]{:S(2)}) copy-start(bf16[384,2,64]{0,2,1:T(8,128)(2,1)} %get-tuple-element.30) | copy-start | bytes 294916 | tf_op jit(solution)/shard_map/cond
  124.0 2.5 %copy-start.1 = (bf16[3072,512]{1,0:T(8,128)(2,1)S(1)}, bf16[3072,512]{1,0:T(8,128)(2,1)}, u32[]{:S(2)}) copy-start(bf16[3072,512]{1,0:T(8,128)(2,1)} %get-tuple-element.26) | copy-start | bytes 9437188 | tf_op jit(solution)/shard_map/cond
  124.0 2.5 %copy-start.15 = (bf16[512,256]{1,0:T(8,128)(2,1)S(1)}, bf16[512,256]{1,0:T(8,128)(2,1)}, u32[]{:S(2)}) copy-start(bf16[512,256]{1,0:T(8,128)(2,1)} %get-tuple-element.39) | copy-start | bytes 786436 | tf_op jit(solution)/shard_map/cond
  133.8 9.9 %copy-start.6 = (bf16[4,256,512]{2,1,0:T(8,128)(2,1)S(1)}, bf16[4,256,512]{2,1,0:T(8,128)(2,1)}, u32[]{:S(2)}) copy-start(bf16[4,256,512]{2,1,0:T(8,128)(2,1)} %copy.59) | copy-start | bytes 3145732
  143.6 2.7 %copy-start.7 = (bf16[384,1024]{0,1:T(8,128)(2,1)S(1)}, bf16[384,1024]{0,1:T(8,128)(2,1)}, u32[]{:S(2)}) copy-start(bf16[384,1024]{0,1:T(8,128)(2,1)} %all_gather.16) | copy-start | bytes 2359300
Sparse Core Ops, SparseCore 0:
  8.9 29.3 all-gather.2
  46.3 66.8 all-gather.4
